TPU v7x, 256 devices: a whole 4x4x8 slice. The times are simulated.
256 devices in a mesh: sp: 32 (over z, x), tp: 8 (over y, core).
Axes of the slice: x: 4, y: 4, z: 8, core: 2. Of those that a mesh axis runs over, the one named last changes fastest.
Arguments:
- tokens: bfloat16 [2, 6144, 4096], P(None, 'sp', 'tp'), may hold values from -12 to 12
- query_weight: bfloat16 [4096, 2048], P(None, 'tp'), may hold values from -0.09375 to 0.09375
- key_weight: bfloat16 [4096, 2048], P(None, 'tp'), may hold values from -0.09375 to 0.09375
- value_weight: bfloat16 [4096, 2048], P(None, 'tp'), may hold values from -0.09375 to 0.09375
- gate_weight: bfloat16 [4096, 2048], P(None, 'tp'), may hold values from -0.09375 to 0.09375
- beta_weight: bfloat16 [4096, 16], P(None, 'tp'), may hold values from -0.09375 to 0.09375
- decay_weight: bfloat16 [4096, 16], P(None, 'tp'), may hold values from -0.09375 to 0.09375
- beta_bias: float32 [16], P('tp'), may hold values from -6 to -3
- rate_log: float32 [16], P('tp'), may hold values from -12 to -2.5
- out_gain: float32 [128], replicated, may hold values from 0.1 to 1.9
- new_query: bfloat16 [2, 16, 128], P(None, 'tp'), may hold values from -6 to 6
- new_key: bfloat16 [2, 16, 128], P(None, 'tp'), may hold values from -6 to 6
- new_value: bfloat16 [2, 16, 128], P(None, 'tp'), may hold values from -6 to 6
- new_beta: float32 [2, 16], P(None, 'tp'), may hold values from 0.1 to 0.9
- new_decay: float32 [2, 16], P(None, 'tp'), may hold values from 0.3 to 1
Outputs:
- mixed_out: bfloat16 [2, 6144, 2048], P(None, 'sp', 'tp')
- cache: bfloat16 [2, 16, 128, 128], P(None, 'tp', 'sp')
- first_out: float32 [2, 2048], P(None, 'tp')
All inputs are finite; a program needn't handle non-finite values.
Results may differ from a plain program's by a relative error of at most 0.0073.
Values may be sent and summed in bfloat16 or wider, within the bound.
No kernel may reach another device: no remote copies, remote signals or barrier semaphores. Data moves between devices by JAX's collectives and lax.ppermute only.
A program may use at most 64 MiB of HBM per device.

v0:
```python
import jax
import jax.numpy as jnp
from jax import lax
from jax.sharding import Mesh
from jax.sharding import PartitionSpec as P

BLOCK = 64
SP = ("sp_0", "sp_1")
unit_floor = 1.0
norm_floor = 0.001
highest = lax.Precision.HIGHEST


def neutral_like(value, identity):
    return jax.tree.map(
        lambda a, e: jnp.broadcast_to(jnp.asarray(e, a.dtype), a.shape), value, identity
    )


def carried_in(value, axes, combine, identity):
    before = start = neutral_like(value, identity)
    subtotal = value
    for axis in reversed(axes):
        length, index = (lax.axis_size(axis), lax.axis_index(axis))
        pieces = jax.tree.map(lambda part: lax.all_gather(part, axis), subtotal)
        inside, subtotal = (start, start)
        for k in range(length):
            passed = k < index
            subtotal = combine(subtotal, jax.tree.map(lambda part: part[k], pieces))
            inside = jax.tree.map(lambda new, old: jnp.where(passed, new, old), subtotal, inside)
        before = combine(inside, before)
    return before


def split_up(value, dim, length):
    before, after = (value.shape[:dim], value.shape[dim + 1 :])
    return jnp.moveaxis(value.reshape(*before, length, -1, *after), dim, 0)


def summed_on_arrival(value, axis, dim):
    parts = split_up(value, dim, lax.axis_size(axis))
    arrived = lax.all_to_all(parts, axis, split_axis=0, concat_axis=0, tiled=True)
    return arrived.astype(jnp.float32).sum(axis=0)


def copy_for_each(value, axis):
    length = lax.axis_size(axis)
    return lax.all_to_all(
        jnp.broadcast_to(value[None], (length, *value.shape)), axis, 0, 0, tiled=True
    )


def over_copies(value, axis):
    everything = copy_for_each(value, axis)
    return jnp.sum(everything, axis=0)


def in_one(arrays, axis):
    ravelled, at, gathered = (jnp.concatenate([a.reshape(-1) for a in arrays]), 0, [])
    subtotal = over_copies(ravelled, axis)
    for a in arrays:
        gathered.append(subtotal[at : at + a.size].reshape(a.shape))
        at += a.size
    return tuple(gathered)


def matmul(form, left, right):
    return jnp.einsum(form, left, right, precision=highest)


def unit_rows(values):
    return values * lax.rsqrt(jnp.sum(values * values, axis=-1, keepdims=True) + unit_floor)


def head_norm(values, out_gain):
    return (
        values
        * lax.rsqrt(jnp.mean(values * values, axis=-1, keepdims=True) + norm_floor)
        * out_gain
    )


def stored(values):
    return lax.optimization_barrier(values.astype(jnp.bfloat16)).astype(jnp.float32)


def unit_lower_inverse(lower_part):
    extent = lower_part.shape[-1]
    nilpotent = -lower_part
    inverse = jnp.eye(extent, dtype=jnp.float32) + nilpotent
    for _ in range(extent.bit_length() - 2):
        nilpotent = matmul("...ij,...jk->...ik", nilpotent, nilpotent)
        inverse = inverse + matmul("...ij,...jk->...ik", nilpotent, inverse)
    return inverse


def prepare(
    query_rows,
    key_rows,
    value_rows,
    beta_in,
    decay_in,
    beta_bias,
    rate_log,
    seq_count,
    length,
    head_count,
):
    extent = query_rows.shape[-1] // head_count
    blocks = length // BLOCK

    def by_head(values):
        shaped = values.reshape(seq_count, blocks, BLOCK, head_count, extent)
        return shaped.transpose(0, 3, 1, 2, 4).reshape(
            seq_count * head_count, blocks, BLOCK, extent
        )

    def by_scalar(values):
        shaped = values.reshape(seq_count, blocks, BLOCK, head_count)
        return shaped.transpose(0, 3, 1, 2).reshape(seq_count * head_count, blocks, BLOCK)

    queries = unit_rows(by_head(query_rows))
    key_unit = unit_rows(by_head(key_rows))
    values = by_head(value_rows)
    strength = by_scalar(jax.nn.sigmoid(beta_in + beta_bias))
    decays = by_scalar(-jnp.exp(rate_log) * jax.nn.softplus(decay_in))
    return (queries, key_unit, values, strength, decays)


def block_terms(queries, key_unit, values, strength, decays):
    extent = decays.shape[-1]
    cumulative = jnp.cumsum(decays, axis=-1)
    causal = jnp.tril(jnp.ones((extent, extent), bool))
    strict = jnp.tril(jnp.ones((extent, extent), bool), -1)
    spread = cumulative[..., :, None] - cumulative[..., None, :]
    weights = jnp.where(causal, jnp.exp(jnp.where(causal, spread, 0.0)), 0.0)
    key_beta = key_unit * strength[..., None]
    lower_part = jnp.where(strict, matmul("...td,...sd->...ts", key_beta, key_unit) * weights, 0.0)
    inverse = unit_lower_inverse(lower_part)
    update = matmul("...ts,...se->...te", inverse, values * strength[..., None])
    carry_w = matmul("...ts,...sd->...td", inverse, key_beta * jnp.exp(cumulative)[..., None])
    scores = matmul("...td,...sd->...ts", queries, key_unit) * weights
    query_decay = queries * jnp.exp(cumulative)[..., None]
    last_log = cumulative[..., -1]
    key_decay = key_unit * jnp.exp(last_log[..., None] - cumulative)[..., None]
    return (update, carry_w, query_decay, scores, key_decay, last_log)


def finish_read(recall, retrieve, query_unit, key_unit, new_value, new_beta, new_decay, out_gain):
    seq_count, head_count, extent = recall.shape
    intersect = jnp.sum(key_unit * query_unit, axis=-1)
    fresh_values = new_value.astype(jnp.float32) - new_decay[..., None] * retrieve
    read_heads = new_decay[..., None] * recall + (new_beta * intersect)[..., None] * fresh_values
    return head_norm(read_heads, out_gain).reshape(seq_count, head_count * extent)


def project_rows(shard_rows, weights):
    row_count = shard_rows.shape[-1]
    flat_rows = shard_rows.reshape(-1, row_count)
    return tuple(
        (jnp.dot(flat_rows, weight, preferred_element_type=jnp.float32) for weight in weights)
    )


def shards(
    tokens,
    query_weight,
    key_weight,
    value_weight,
    gate_weight,
    beta_weight,
    decay_weight,
    beta_bias,
    rate_log,
    out_gain,
    new_query,
    new_key,
    new_value,
    new_beta,
    new_decay,
):
    seq_count, span_len, _ = tokens.shape
    head_count = rate_log.shape[0]
    weights = (query_weight, key_weight, value_weight, gate_weight, beta_weight, decay_weight)
    totals = project_rows(lax.all_gather(tokens, "tp", axis=2, tiled=True), weights)
    query_rows = stored(totals[0])
    key_rows = stored(totals[1])
    value_rows = stored(totals[2])
    gate_rows = stored(totals[3])
    prepared = prepare(
        query_rows,
        key_rows,
        value_rows,
        totals[4],
        totals[5],
        beta_bias,
        rate_log,
        seq_count,
        span_len,
        head_count,
    )
    block_data = block_terms(*prepared)
    batch_size = block_data[0].shape[0]
    extent = block_data[0].shape[-1]
    identity = jnp.broadcast_to(jnp.eye(extent, dtype=jnp.float32), (batch_size, extent, extent))

    def advance(carried, inputs):
        state_now, reach_map = carried
        u_block, w_block, qg_block, score_block, kd_block, gl_block = inputs
        fresh_values = u_block - matmul("btd,bde->bte", w_block, state_now)
        block_out = matmul("btd,bde->bte", qg_block, state_now) + matmul(
            "bts,bse->bte", score_block, fresh_values
        )
        reach_rows = qg_block - matmul("bts,bsd->btd", score_block, w_block)
        factor = jnp.exp(gl_block)[:, None, None]
        transit = factor * identity - matmul("bsd,bse->bde", kd_block, w_block)
        state_next = state_now * factor + matmul("bsd,bse->bde", kd_block, fresh_values)
        map_next = matmul("bde,bef->bdf", transit, reach_map)
        return ((state_next, map_next), (block_out, matmul("btd,bde->bte", reach_rows, reach_map)))

    inputs = tuple((jnp.moveaxis(member, 1, 0) for member in block_data))
    start_state = jnp.zeros((batch_size, extent, extent), jnp.float32)
    (local_state, local_map), (local_out, reach_all) = lax.scan(
        advance, (start_state, identity), inputs
    )

    def compose(earlier, later):
        return (
            matmul("bde,bef->bdf", later[0], earlier[0]),
            matmul("bde,bef->bdf", later[0], earlier[1]) + later[1],
        )

    prefix = carried_in(
        (local_map, local_state), SP, compose, (identity, jnp.zeros_like(local_state))
    )
    incoming = prefix[1]
    block_total = local_out + matmul("nbtd,bde->nbte", reach_all, incoming)
    blocks = span_len // BLOCK
    heads_out = block_total.reshape(blocks, seq_count, head_count, BLOCK, extent).transpose(
        1, 0, 3, 2, 4
    )
    heads_out = heads_out.reshape(seq_count, span_len, head_count, extent)
    gate_values = gate_rows.reshape(seq_count, span_len, head_count, extent)
    mixed_out = (head_norm(heads_out, out_gain) * jax.nn.silu(gate_values)).astype(jnp.bfloat16)
    mixed_out = mixed_out.reshape(seq_count, span_len, head_count * extent)
    final_state = matmul("bde,bef->bdf", local_map, incoming) + local_state
    final_cast = final_state.reshape(seq_count, head_count, extent, extent).astype(jnp.bfloat16)
    row_count = extent // lax.axis_size(SP)
    row_start = lax.axis_index(SP) * row_count
    query_unit = unit_rows(new_query.astype(jnp.float32))
    key_unit = unit_rows(new_key.astype(jnp.float32))
    is_last = lax.axis_index(SP) == lax.axis_size(SP) - 1
    own_term = jnp.where(is_last, final_cast.astype(jnp.float32), 0.0)
    cache_rows = summed_on_arrival(own_term.astype(jnp.bfloat16), SP, 2).astype(jnp.bfloat16)
    memory = lax.optimization_barrier(cache_rows).astype(jnp.float32)
    query_part = lax.dynamic_slice_in_dim(query_unit, row_start, row_count, 2)
    key_part = lax.dynamic_slice_in_dim(key_unit, row_start, row_count, 2)
    recall, retrieve = in_one(
        (matmul("shde,shd->she", memory, query_part), matmul("shde,shd->she", memory, key_part)), SP
    )
    first_out = finish_read(
        recall, retrieve, query_unit, key_unit, new_value, new_beta, new_decay, out_gain
    )
    return (mixed_out, cache_rows, first_out)


def solution(mesh):
    torus = Mesh(mesh.devices.reshape(8, 4, mesh.shape["tp"]), ("sp_0", "sp_1", "tp"))
    in_specs = (
        P(None, SP, "tp"),
        P(None, "tp"),
        P(None, "tp"),
        P(None, "tp"),
        P(None, "tp"),
        P(None, "tp"),
        P(None, "tp"),
        P("tp"),
        P("tp"),
        P(),
        P(None, "tp", None),
        P(None, "tp", None),
        P(None, "tp", None),
        P(None, "tp"),
        P(None, "tp"),
    )
    out_specs = (P(None, SP, "tp"), P(None, "tp", SP, None), P(None, "tp"))
    return jax.shard_map(
        shards, mesh=torus, in_specs=in_specs, out_specs=out_specs, check_vma=False
    )
```

profile of v0, /device:TPU:8, one launch (start us, length us, event | category | flops | bytes accessed | tf_op | source)
XLA Modules:
  0.0 295.3 jit_solution(3390538268324986770)
XLA Ops:
  9.4 32.6 %all-gather.10.cloned.1.call-done = bf16[2,192,4096]{2,1,0:T(8,128)(2,1)} async-done(((bf16[2,192,512]{2,1,0:T(8,128)(2,1)}), bf16[2,192,4096]{2,1,0:T(8,128)(2,1)}) %all-gather.10.cloned.1.call-update) | async-done | bytes 3145744 | tf_op jit(solution)/shard_map/all_gather | solution.py:185
  42.0 2.8 fusion.91
  46.8 2.9 convolution_convert_fusion.1
  51.3 2.8 fusion.50
  54.3 3.5 %convolution_convert_fusion.3 = bf16[384,256]{1,0:T(8,128)(2,1)S(1)} fusion(bf16[384,4096]{1,0:T(8,128)(2,1)} %bitcast.236, bf16[4096,256]{1,0:T(8,128)(2,1)} %param.19), kind=kOutput, calls=%fused_computation.61 | convolution fusion | flops 805404672 | bytes 5439488 | tf_op jit(solution)/shard_map/dot_general | solution.py:161
  59.4 3.6 %convolution_convert_fusion.2 = bf16[384,256]{1,0:T(8,128)(2,1)S(1)} fusion(bf16[384,4096]{1,0:T(8,128)(2,1)} %bitcast.237, bf16[4096,256]{1,0:T(8,128)(2,1)} %param.20), kind=kOutput, calls=%fused_computation.60 | convolution fusion | flops 805404672 | bytes 5439488 | tf_op jit(solution)/shard_map/dot_general | solution.py:161
  73.8 1.5 fusion.39
  75.3 29.5 %while.17 = (s32[]{:T(128)}, f32[4,128,128]{2,1,0:T(8,128)S(1)}, f32[4,128,128]{2,1,0:T(8,128)S(1)}, f32[3,4,64,128]{3,2,0,1:T(8,128)}, f32[3,4,64,128]{3,2,0,1:...) while((s32[]{:T(128)}, f32[4,128,128]{2,1,0:T(8,128)S(1)}, ...), condition=%wide.region_4.5_spmd.clone, body=%wide.region_3.4_spmd.clone.sunk | while | flops 403210240 | bytes 5445847 | solution.py:223
  79.5 1.5 convolution_add_fusion.23
  83.2 1.5 convolution_subtract_fusion.7
  89.3 1.5 convolution_add_fusion.23
  99.2 1.5 convolution_add_fusion.23
  106.4 26.9 %all-gather.12.cloned.1.call-done = f32[16,128,128]{2,1,0:T(8,128)} async-done(((f32[4,128,128]{2,1,0:T(8,128)}), f32[16,128,128]{2,1,0:T(8,128)}) %all-gather.12.cloned.1.call-update) | async-done | bytes 1048592 | tf_op jit(solution)/shard_map/all_gather | solution.py:25
  139.8 22.4 %all-gather.16.cloned.1.call-done = f32[16,128,128]{2,1,0:T(8,128)} async-done(((f32[4,128,128]{2,1,0:T(8,128)}), f32[16,128,128]{2,1,0:T(8,128)}) %all-gather.16.cloned.1.call-update) | async-done | bytes 1048592 | tf_op jit(solution)/shard_map/all_gather | solution.py:25
  168.5 4.3 %convolution_convert_fusion = bf16[384,256]{1,0:T(8,128)(2,1)} fusion(bf16[384,4096]{1,0:T(8,128)(2,1)} %bitcast.238, bf16[4096,256]{1,0:T(8,128)(2,1)} %param.21), kind=kOutput, calls=%fused_computation.58 | convolution fusion | flops 805404672 | bytes 5439488 | tf_op jit(solution)/shard_map/dot_general | solution.py:161
  173.9 31.2 %all-gather.14.cloned.1.call-done = f32[32,128,128]{2,1,0:T(8,128)} async-done(((f32[4,128,128]{2,1,0:T(8,128)}), f32[32,128,128]{2,1,0:T(8,128)}) %all-gather.14.cloned.1.call-update) | async-done | bytes 2097168 | tf_op jit(solution)/shard_map/all_gather | solution.py:25
  205.1 41.1 %all-gather.18.cloned.1.call-done = f32[32,128,128]{2,1,0:T(8,128)} async-done(((f32[4,128,128]{2,1,0:T(8,128)}), f32[32,128,128]{2,1,0:T(8,128)}) %all-gather.18.cloned.1.call-update) | async-done | bytes 2097168 | tf_op jit(solution)/shard_map/all_gather | solution.py:25
  246.2 1.5 convolution_add_fusion.20
  254.7 7.1 %all-to-all-start = ((bf16[32,2,2,4,128]{4,3,2,1,0:T(4,128)(2,1)}), bf16[32,2,2,4,128]{4,3,2,1,0:T(4,128)(2,1)S(1)}, u32[]{:S(2)}, u32[]{:S(2)}) async-start(bf16[32,2,2,4,128]{4,3,2,1,0:T(4,128)(2,1)} %bitcast.193), calls=%async_computation | async-start | bytes 262144 | tf_op jit(solution)/shard_map/all_to_all | solution.py:42
  261.8 1.6 fusion.38
  265.2 7.1 %all-to-all-done = bf16[32,2,2,4,128]{4,3,2,1,0:T(4,128)(2,1)S(1)} async-done(((bf16[32,2,2,4,128]{4,3,2,1,0:T(4,128)(2,1)}), bf16[32,2,2,4,128]{4,3,2,1,0:T(4,128)(2,1)S(1)}, u32[]{:S(2)}, u32[]{:S(2)}) %all-to-all-start) | async-done | bytes 131104 | tf_op jit(solution)/shard_map/all_to_all | solution.py:42
  273.4 3.8 %all-to-all-start.1 = ((f32[32,1,1024]{2,1,0:T(1,128)}), f32[32,1,1024]{2,1,0:T(1,128)S(1)}, u32[]{:S(2)}, u32[]{:S(2)}) async-start(f32[32,1,1024]{2,1,0:T(1,128)} %broadcast_in_dim.80), calls=%async_computation.1 | async-start | bytes 262144 | tf_op jit(solution)/shard_map/all_to_all | solution.py:48
  277.3 1.7 fusion.60
  279.0 8.8 %all-to-all-done.1 = f32[32,1,1024]{2,1,0:T(1,128)S(1)} async-done(((f32[32,1,1024]{2,1,0:T(1,128)}), f32[32,1,1024]{2,1,0:T(1,128)S(1)}, u32[]{:S(2)}, u32[]{:S(2)}) %all-to-all-start.1) | async-done | bytes 131104 | tf_op jit(solution)/shard_map/all_to_all | solution.py:48
  (195 shorter events, 67.1 us)
Async XLA Ops:
  7.2 39.7 %copy-start = (bf16[4096,256]{1,0:T(8,128)(2,1)S(1)}, bf16[4096,256]{1,0:T(8,128)(2,1)}, u32[]{:S(2)}) copy-start(bf16[4096,256]{1,0:T(8,128)(2,1)} %param.18) | copy-start | bytes 6291460
  7.2 34.8 %all-gather.10.cloned.1.call-start = ((), (), s32[]{:S(2)}) async-start(), calls=%async_computation.2 | async-start | bytes 3538944 | tf_op jit(solution)/shard_map/all_gather | solution.py:185
  7.9 125.4 %all-gather.12.cloned.1.call-start = ((), (), s32[]{:S(2)}) async-start(), calls=%async_computation.3 | async-start | bytes 1310720 | tf_op jit(solution)/shard_map/all_gather | solution.py:25
  59.4 3.8 %copy-start.20 = (f32[2,2,3,64,128]{4,3,1,0,2:T(8,128)S(1)}, f32[2,2,3,64,128]{4,3,1,0,2:T(8,128)}, u32[]{:S(2)}) copy-start(f32[2,2,3,64,128]{4,3,1,0,2:T(8,128)} %copy.189) | copy-start | bytes 1179652
  105.6 56.6 %all-gather.16.cloned.1.call-start = ((), (), s32[]{:S(2)}) async-start(), calls=%async_computation.5 | async-start | bytes 1310720 | tf_op jit(solution)/shard_map/all_gather | solution.py:25
  106.3 98.8 %all-gather.14.cloned.1.call-start = ((), (), s32[]{:S(2)}) async-start(), calls=%async_computation.4 | async-start | bytes 2359296 | tf_op jit(solution)/shard_map/all_gather | solution.py:25
  133.3 4.2 %copy-start.3 = (f32[16,128,128]{2,1,0:T(8,128)S(1)}, f32[16,128,128]{2,1,0:T(8,128)}, u32[]{:S(2)}) copy-start(f32[16,128,128]{2,1,0:T(8,128)} %all-gather.12.cloned.1.call-done) | copy-start | bytes 3145732
  139.7 106.4 %all-gather.18.cloned.1.call-start = ((), (), s32[]{:S(2)}) async-start(), calls=%async_computation.6 | async-start | bytes 2359296 | tf_op jit(solution)/shard_map/all_gather | solution.py:25
  162.2 3.5 %copy-start.22 = (f32[16,128,128]{2,1,0:T(8,128)S(1)}, f32[16,128,128]{2,1,0:T(8,128)}, u32[]{:S(2)}) copy-start(f32[16,128,128]{2,1,0:T(8,128)} %all-gather.16.cloned.1.call-done) | copy-start | bytes 3145732
  163.6 4.4 %copy-start.26 = (bf16[2,2,128]{2,1,0:T(2,128)(2,1)S(1)}, bf16[2,2,128]{2,1,0:T(2,128)(2,1)}, u32[]{:S(2)}) copy-start(bf16[2,2,128]{2,1,0:T(2,128)(2,1)} %param.27) | copy-start | bytes 3076
  163.6 4.5 %copy-start.27 = (bf16[2,2,128]{2,1,0:T(2,128)(2,1)S(1)}, bf16[2,2,128]{2,1,0:T(2,128)(2,1)}, u32[]{:S(2)}) copy-start(bf16[2,2,128]{2,1,0:T(2,128)(2,1)} %param.28) | copy-start | bytes 3076
  163.6 4.7 %copy-start.29 = (f32[2,2]{1,0:T(2,128)S(1)}, f32[2,2]{1,0:T(2,128)}, u32[]{:S(2)}) copy-start(f32[2,2]{1,0:T(2,128)} %param.30) | copy-start | bytes 52
  163.6 4.8 %copy-start.32 = (f32[128]{0:T(128)S(1)}, f32[128]{0:T(128)}, u32[]{:S(2)}) copy-start(f32[128]{0:T(128)} %param.26) | copy-start | bytes 1540
  168.4 4.3 %copy-start.8 = (f32[4,128,128]{2,1,0:T(8,128)S(1)}, f32[4,128,128]{2,1,0:T(8,128)}, u32[]{:S(2)}) copy-start(f32[4,128,128]{2,1,0:T(8,128)} %copy-done.7) | copy-start | bytes 786436
  168.4 4.3 %copy-start.10 = (f32[4,128,128]{2,1,0:T(8,128)S(1)}, f32[4,128,128]{2,1,0:T(8,128)}, u32[]{:S(2)}) copy-start(f32[4,128,128]{2,1,0:T(8,128)} %copy-done.9) | copy-start | bytes 786436
  168.4 4.3 %copy-start.12 = (f32[4,128,128]{2,1,0:T(8,128)S(1)}, f32[4,128,128]{2,1,0:T(8,128)}, u32[]{:S(2)}) copy-start(f32[4,128,128]{2,1,0:T(8,128)} %fusion.109) | copy-start | bytes 786436
  168.4 4.3 %copy-start.18 = (f32[4,128,128]{2,1,0:T(8,128)S(1)}, f32[4,128,128]{2,1,0:T(8,128)}, u32[]{:S(2)}) copy-start(f32[4,128,128]{2,1,0:T(8,128)} %copy-done.17) | copy-start | bytes 786436
  246.2 3.0 %copy-start.6 = (f32[32,128,128]{2,1,0:T(8,128)S(1)}, f32[32,128,128]{2,1,0:T(8,128)}, u32[]{:S(2)}) copy-start(f32[32,128,128]{2,1,0:T(8,128)} %all-gather.14.cloned.1.call-done) | copy-start | bytes 6291460
  246.2 4.3 %copy-start.19 = (f32[32,128,128]{2,1,0:T(8,128)S(1)}, f32[32,128,128]{2,1,0:T(8,128)}, u32[]{:S(2)}) copy-start(f32[32,128,128]{2,1,0:T(8,128)} %all-gather.18.cloned.1.call-done) | copy-start | bytes 6291460
  254.7 17.6 %all-to-all-start = ((bf16[32,2,2,4,128]{4,3,2,1,0:T(4,128)(2,1)}), bf16[32,2,2,4,128]{4,3,2,1,0:T(4,128)(2,1)S(1)}, u32[]{:S(2)}, u32[]{:S(2)}) async-start(bf16[32,2,2,4,128]{4,3,2,1,0:T(4,128)(2,1)} %bitcast.193), calls=%async_computation | async-start | bytes 262144 | tf_op jit(solution)/shard_map/all_to_all | solution.py:42
  263.9 24.0 %copy-start.30 = (bf16[2,2,128]{2,1,0:T(2,128)(2,1)S(1)}, bf16[2,2,128]{2,1,0:T(2,128)(2,1)}, u32[]{:S(2)}) copy-start(bf16[2,2,128]{2,1,0:T(2,128)(2,1)} %param.29) | copy-start | bytes 3076
  263.9 24.0 %copy-start.31 = (f32[2,2]{1,0:T(2,128)S(1)}, f32[2,2]{1,0:T(2,128)}, u32[]{:S(2)}) copy-start(f32[2,2]{1,0:T(2,128)} %param.31) | copy-start | bytes 52
  272.4 16.4 %copy-start.25 = (bf16[2,2,4,128]{3,2,1,0:T(4,128)(2,1)}, bf16[2,2,4,128]{3,2,1,0:T(4,128)(2,1)S(1)}, u32[]{:S(2)}) copy-start(bf16[2,2,4,128]{3,2,1,0:T(4,128)(2,1)S(1)} %reduce_sum.87) | copy-start | bytes 12292
  273.4 14.4 %all-to-all-start.1 = ((f32[32,1,1024]{2,1,0:T(1,128)}), f32[32,1,1024]{2,1,0:T(1,128)S(1)}, u32[]{:S(2)}, u32[]{:S(2)}) async-start(f32[32,1,1024]{2,1,0:T(1,128)} %broadcast_in_dim.80), calls=%async_computation.1 | async-start | bytes 262144 | tf_op jit(solution)/shard_map/all_to_all | solution.py:48
  (16 other events, 17.8 us)
Sparse Core Ops, SparseCore 0:
  9.8 32.1 all-gather.9
  105.7 27.5 all-gather.11
  135.1 27.0 all-gather.15
  163.8 41.2 all-gather.13
  206.7 39.4 all-gather.17
where the time goes:
time: 296 us; the launch traced here: 295 us
  waiting for transfers between devices  172 us (58%)
  matrix products  75.5 us (26%)
  between operations  14.6 us (5%)
  local copies, waits for them, and re-layouts  13.8 us (5%)
  starting transfers between devices  11.1 us (4%)
  other arithmetic  8.51 us (3%)
    all_gather x4, waiting for transfers between devices, carried_in(): pieces = jax.tree.map(lambda part: lax.all_gather(part, axis), subtotal)  122 us
    dot_general x61, matrix products, matmul(): return jnp.einsum(form, left, right, precision=highest)  55.6 us
    all_gather x1, waiting for transfers between devices, shards(): lax.all_gather(tokens, 'tp', axis=2, tiled=True)  32.6 us
    dot_general x6, matrix products, project_rows(): jnp.dot(flat_rows, weight, preferred_element_type=jnp.float32)  19.9 us
    all_to_all x1, waiting for transfers between devices, copy_for_each(): lax.all_to_all(jnp.broadcast_to(value[None], (length, *value.shape)), axi...  8.81 us
    all_to_all x1, waiting for transfers between devices, summed_on_arrival(): lax.all_to_all(parts, axis, split_axis=0, concat_axis=0, tiled=True)  7.1 us
    all_to_all x1, starting transfers between devices, summed_on_arrival(): lax.all_to_all(parts, axis, split_axis=0, concat_axis=0, tiled=True)  7.08 us
  transfers between devices with their start and end apart: 7, of which 7 were waited for; matrix products, arithmetic and copies ran while one was open for 7% of the time, Pallas kernels for 0%

commit v1 on v0

--- a/solution.py
+++ b/solution.py
@@ -182,7 +182,12 @@
     seq_count, span_len, _ = tokens.shape
     head_count = rate_log.shape[0]
     weights = (query_weight, key_weight, value_weight, gate_weight, beta_weight, decay_weight)
-    totals = project_rows(lax.all_gather(tokens, "tp", axis=2, tiled=True), weights)
+    totals = project_rows(
+        jnp.concatenate(
+            lax.all_to_all(jnp.stack([tokens] * lax.axis_size("tp")), "tp", 0, 0), axis=2
+        ),
+        weights,
+    )
     query_rows = stored(totals[0])
     key_rows = stored(totals[1])
     value_rows = stored(totals[2])

time: 296 us -> 314 us (1.061)
  local copies, waits for them, and re-layouts: 13.8 us -> 23.1 us
  starting transfers between devices: 11.1 us -> 17.8 us
    all_to_all x0 -> x1, waiting for transfers between devices: none -> 36.3 us  [shards(): lax.all_to_all(jnp.stack([tokens] * lax.axis_size('tp')), 'tp', 0, 0)]
    all_gather x1 -> x0, waiting for transfers between devices: 32.6 us -> none  [shards(): lax.all_gather(tokens, 'tp', axis=2, tiled=True)]
    all_to_all x0 -> x1, starting transfers between devices: none -> 6.63 us  [shards(): lax.all_to_all(jnp.stack([tokens] * lax.axis_size('tp')), 'tp', 0, 0)]
    reshape x0 -> x1, local copies, waits for them, and re-layouts: none -> 3.64 us  [shards(): jnp.concatenate(lax.all_to_all(jnp.stack([tokens] * lax.axis_size('tp')),...]
    unnamed x68 -> x81, local copies, waits for them, and re-layouts: 5.89 us -> 8.38 us
  transfers between devices with their start and end apart: 7 -> 7, of which waited for: 7 -> 7; matrix products, arithmetic and copies ran while one was open for 7% -> 6% of each run, Pallas kernels for 0% -> 0%
where the time goes in v1:
time: 314 us; the launch traced here: 313 us
  waiting for transfers between devices  174 us (55%)
  matrix products  73.8 us (24%)
  local copies, waits for them, and re-layouts  23.1 us (7%)
  starting transfers between devices  17.8 us (6%)
  between operations  14.6 us (5%)
  other arithmetic  8.87 us (3%)
    all_gather x4, waiting for transfers between devices, carried_in(): pieces = jax.tree.map(lambda part: lax.all_gather(part, axis), subtotal)  122 us
    dot_general x61, matrix products, matmul(): return jnp.einsum(form, left, right, precision=highest)  55.8 us
    all_to_all x1, waiting for transfers between devices, shards(): lax.all_to_all(jnp.stack([tokens] * lax.axis_size('tp')), 'tp', 0, 0)  36.3 us
    dot_general x6, matrix products, project_rows(): jnp.dot(flat_rows, weight, preferred_element_type=jnp.float32)  18 us
    all_to_all x1, waiting for transfers between devices, copy_for_each(): lax.all_to_all(jnp.broadcast_to(value[None], (length, *value.shape)), axi...  8.81 us
    unnamed x81, local copies, waits for them, and re-layouts  8.38 us
    all_to_all x1, starting transfers between devices, summed_on_arrival(): lax.all_to_all(parts, axis, split_axis=0, concat_axis=0, tiled=True)  7.2 us
    all_to_all x1, waiting for transfers between devices, summed_on_arrival(): lax.all_to_all(parts, axis, split_axis=0, concat_axis=0, tiled=True)  7.07 us
  transfers between devices with their start and end apart: 7, of which 7 were waited for; matrix products, arithmetic and copies ran while one was open for 6% of the time, Pallas kernels for 0%

profile of v1, /device:TPU:8, one launch (start us, length us, event | category | flops | bytes accessed | tf_op | source)
XLA Modules:
  0.0 313.0 jit_solution(3897987379828684881)
XLA Ops:
  7.2 3.1 %stack.2 = bf16[8,2,192,512]{3,2,1,0:T(8,128)(2,1)} broadcast(bf16[2,192,512]{2,1,0:T(8,128)(2,1)} %param.17), dimensions={1,2,3} | broadcast | bytes 3538944 | tf_op jit(solution)/shard_map/stack | solution.py:187
  10.3 6.6 %all-to-all-start = ((bf16[8,2,192,512]{3,2,1,0:T(8,128)(2,1)}), bf16[8,2,192,512]{3,2,1,0:T(8,128)(2,1)}, u32[]{:S(2)}, u32[]{:S(2)}) async-start(bf16[8,2,192,512]{3,2,1,0:T(8,128)(2,1)} %stack.2), calls=%async_computation | async-start | bytes 6291456 | tf_op jit(solution)/shard_map/all_to_all | solution.py:187
  17.7 36.3 %all-to-all-done = bf16[8,2,192,512]{3,2,1,0:T(8,128)(2,1)} async-done(((bf16[8,2,192,512]{3,2,1,0:T(8,128)(2,1)}), bf16[8,2,192,512]{3,2,1,0:T(8,128)(2,1)}, u32[]{:S(2)}, u32[]{:S(2)}) %all-to-all-start) | async-done | bytes 3145760 | tf_op jit(solution)/shard_map/all_to_all | solution.py:187
  54.0 3.6 %copy.180 = bf16[2,192,8,512]{3,2,1,0:T(8,128)(2,1)S(1)} copy(bf16[2,192,8,512]{3,1,0,2:T(8,128)(2,1)} %bitcast) | data formatting | bytes 6291456 | tf_op jit(solution)/shard_map/reshape | solution.py:186
  59.1 1.6 copy-done.3
  63.8 2.9 convolution_convert_fusion.1
  68.3 2.8 fusion.50
  71.2 3.5 %convolution_convert_fusion.3 = bf16[384,256]{1,0:T(8,128)(2,1)S(1)} fusion(bf16[384,4096]{1,0:T(8,128)(2,1)} %bitcast.239, bf16[4096,256]{1,0:T(8,128)(2,1)} %param.19), kind=kOutput, calls=%fused_computation.61 | convolution fusion | flops 805404672 | bytes 5439488 | tf_op jit(solution)/shard_map/dot_general | solution.py:161
  76.4 3.6 %convolution_convert_fusion.2 = bf16[384,256]{1,0:T(8,128)(2,1)S(1)} fusion(bf16[384,4096]{1,0:T(8,128)(2,1)} %bitcast.240, bf16[4096,256]{1,0:T(8,128)(2,1)} %param.20), kind=kOutput, calls=%fused_computation.60 | convolution fusion | flops 805404672 | bytes 5439488 | tf_op jit(solution)/shard_map/dot_general | solution.py:161
  90.7 1.5 fusion.39
  92.3 29.6 %while.17 = (s32[]{:T(128)}, f32[4,128,128]{2,1,0:T(8,128)S(1)}, f32[4,128,128]{2,1,0:T(8,128)S(1)}, f32[3,4,64,128]{3,2,0,1:T(8,128)}, f32[3,4,64,128]{3,2,0,1:...) while((s32[]{:T(128)}, f32[4,128,128]{2,1,0:T(8,128)S(1)}, ...), condition=%wide.region_4.5_spmd.clone, body=%wide.region_3.4_spmd.clone.sunk | while | flops 403210240 | bytes 5445847 | solution.py:228
  116.2 1.5 convolution_add_fusion.23
  123.4 26.2 %all-gather.9.cloned.1.call-done = f32[16,128,128]{2,1,0:T(8,128)} async-done(((f32[4,128,128]{2,1,0:T(8,128)}), f32[16,128,128]{2,1,0:T(8,128)}) %all-gather.9.cloned.1.call-update) | async-done | bytes 1048592 | tf_op jit(solution)/shard_map/all_gather | solution.py:25
  155.5 23.0 %all-gather.13.cloned.1.call-done = f32[16,128,128]{2,1,0:T(8,128)} async-done(((f32[4,128,128]{2,1,0:T(8,128)}), f32[16,128,128]{2,1,0:T(8,128)}) %all-gather.13.cloned.1.call-update) | async-done | bytes 1048592 | tf_op jit(solution)/shard_map/all_gather | solution.py:25
  185.0 4.3 %convolution_convert_fusion = bf16[384,256]{1,0:T(8,128)(2,1)} fusion(bf16[384,4096]{1,0:T(8,128)(2,1)} %bitcast.241, bf16[4096,256]{1,0:T(8,128)(2,1)} %param.21), kind=kOutput, calls=%fused_computation.58 | convolution fusion | flops 805404672 | bytes 5439488 | tf_op jit(solution)/shard_map/dot_general | solution.py:161
  190.4 31.2 %all-gather.11.cloned.1.call-done = f32[32,128,128]{2,1,0:T(8,128)} async-done(((f32[4,128,128]{2,1,0:T(8,128)}), f32[32,128,128]{2,1,0:T(8,128)}) %all-gather.11.cloned.1.call-update) | async-done | bytes 2097168 | tf_op jit(solution)/shard_map/all_gather | solution.py:25
  221.6 41.1 %all-gather.15.cloned.1.call-done = f32[32,128,128]{2,1,0:T(8,128)} async-done(((f32[4,128,128]{2,1,0:T(8,128)}), f32[32,128,128]{2,1,0:T(8,128)}) %all-gather.15.cloned.1.call-update) | async-done | bytes 2097168 | tf_op jit(solution)/shard_map/all_gather | solution.py:25
  262.7 1.5 convolution_add_fusion.20
  271.4 7.2 %all-to-all-start.1 = ((bf16[32,2,2,4,128]{4,3,2,1,0:T(4,128)(2,1)}), bf16[32,2,2,4,128]{4,3,2,1,0:T(4,128)(2,1)}, u32[]{:S(2)}, u32[]{:S(2)}) async-start(bf16[32,2,2,4,128]{4,3,2,1,0:T(4,128)(2,1)} %bitcast.196), calls=%async_computation.1 | async-start | bytes 262144 | tf_op jit(solution)/shard_map/all_to_all | solution.py:42
  278.6 1.6 fusion.38
  282.0 7.1 %all-to-all-done.1 = bf16[32,2,2,4,128]{4,3,2,1,0:T(4,128)(2,1)} async-done(((bf16[32,2,2,4,128]{4,3,2,1,0:T(4,128)(2,1)}), bf16[32,2,2,4,128]{4,3,2,1,0:T(4,128)(2,1)}, u32[]{:S(2)}, u32[]{:S(2)}) %all-to-all-start.1) | async-done | bytes 131104 | tf_op jit(solution)/shard_map/all_to_all | solution.py:42
  291.0 3.8 %all-to-all-start.2 = ((f32[32,1,1024]{2,1,0:T(1,128)}), f32[32,1,1024]{2,1,0:T(1,128)S(1)}, u32[]{:S(2)}, u32[]{:S(2)}) async-start(f32[32,1,1024]{2,1,0:T(1,128)} %broadcast_in_dim.80), calls=%async_computation.2 | async-start | bytes 262144 | tf_op jit(solution)/shard_map/all_to_all | solution.py:48
  294.9 1.7 fusion.60
  296.6 8.8 %all-to-all-done.2 = f32[32,1,1024]{2,1,0:T(1,128)S(1)} async-done(((f32[32,1,1024]{2,1,0:T(1,128)}), f32[32,1,1024]{2,1,0:T(1,128)S(1)}, u32[]{:S(2)}, u32[]{:S(2)}) %all-to-all-start.2) | async-done | bytes 131104 | tf_op jit(solution)/shard_map/all_to_all | solution.py:48
  (209 shorter events, 73.3 us)
Async XLA Ops:
  7.2 56.6 %copy-start = (bf16[4096,256]{1,0:T(8,128)(2,1)S(1)}, bf16[4096,256]{1,0:T(8,128)(2,1)}, u32[]{:S(2)}) copy-start(bf16[4096,256]{1,0:T(8,128)(2,1)} %param.18) | copy-start | bytes 6291460
  10.3 6.7 %copy-start.38 = (f32[2]{0:T(128)S(1)}, f32[2]{0:T(128)}, u32[]{:S(2)}) copy-start(f32[2]{0:T(128)} %param.25) | copy-start | bytes 28
  10.3 43.7 %all-to-all-start = ((bf16[8,2,192,512]{3,2,1,0:T(8,128)(2,1)}), bf16[8,2,192,512]{3,2,1,0:T(8,128)(2,1)}, u32[]{:S(2)}, u32[]{:S(2)}) async-start(bf16[8,2,192,512]{3,2,1,0:T(8,128)(2,1)} %stack.2), calls=%async_computation | async-start | bytes 6291456 | tf_op jit(solution)/shard_map/all_to_all | solution.py:187
  16.9 132.7 %all-gather.9.cloned.1.call-start = ((), (), s32[]{:S(2)}) async-start(), calls=%async_computation.3 | async-start | bytes 1310720 | tf_op jit(solution)/shard_map/all_gather | solution.py:25
  76.4 3.8 %copy-start.23 = (f32[2,2,3,64,128]{4,3,1,0,2:T(8,128)S(1)}, f32[2,2,3,64,128]{4,3,1,0,2:T(8,128)}, u32[]{:S(2)}) copy-start(f32[2,2,3,64,128]{4,3,1,0,2:T(8,128)} %copy.194) | copy-start | bytes 1179652
  122.6 55.9 %all-gather.13.cloned.1.call-start = ((), (), s32[]{:S(2)}) async-start(), calls=%async_computation.5 | async-start | bytes 1310720 | tf_op jit(solution)/shard_map/all_gather | solution.py:25
  123.4 98.2 %all-gather.11.cloned.1.call-start = ((), (), s32[]{:S(2)}) async-start(), calls=%async_computation.4 | async-start | bytes 2359296 | tf_op jit(solution)/shard_map/all_gather | solution.py:25
  155.4 107.3 %all-gather.15.cloned.1.call-start = ((), (), s32[]{:S(2)}) async-start(), calls=%async_computation.6 | async-start | bytes 2359296 | tf_op jit(solution)/shard_map/all_gather | solution.py:25
  179.9 4.5 %copy-start.8 = (f32[4,128,128]{2,1,0:T(8,128)}, f32[4,128,128]{2,1,0:T(8,128)S(1)}, u32[]{:S(2)}) copy-start(f32[4,128,128]{2,1,0:T(8,128)S(1)} %convolution_add_fusion.19) | copy-start | bytes 786436
  179.9 4.5 %copy-start.30 = (bf16[2,2,128]{2,1,0:T(2,128)(2,1)S(1)}, bf16[2,2,128]{2,1,0:T(2,128)(2,1)}, u32[]{:S(2)}) copy-start(bf16[2,2,128]{2,1,0:T(2,128)(2,1)} %param.27) | copy-start | bytes 3076
  180.0 4.6 %copy-start.31 = (bf16[2,2,128]{2,1,0:T(2,128)(2,1)S(1)}, bf16[2,2,128]{2,1,0:T(2,128)(2,1)}, u32[]{:S(2)}) copy-start(bf16[2,2,128]{2,1,0:T(2,128)(2,1)} %param.28) | copy-start | bytes 3076
  180.0 4.9 %copy-start.33 = (f32[2,2]{1,0:T(2,128)S(1)}, f32[2,2]{1,0:T(2,128)}, u32[]{:S(2)}) copy-start(f32[2,2]{1,0:T(2,128)} %param.30) | copy-start | bytes 52
  180.0 5.0 %copy-start.36 = (f32[128]{0:T(128)S(1)}, f32[128]{0:T(128)}, u32[]{:S(2)}) copy-start(f32[128]{0:T(128)} %param.26) | copy-start | bytes 1540
  184.9 4.3 %copy-start.11 = (f32[4,128,128]{2,1,0:T(8,128)S(1)}, f32[4,128,128]{2,1,0:T(8,128)}, u32[]{:S(2)}) copy-start(f32[4,128,128]{2,1,0:T(8,128)} %copy-done.10) | copy-start | bytes 786436
  184.9 4.3 %copy-start.13 = (f32[4,128,128]{2,1,0:T(8,128)S(1)}, f32[4,128,128]{2,1,0:T(8,128)}, u32[]{:S(2)}) copy-start(f32[4,128,128]{2,1,0:T(8,128)} %copy-done.12) | copy-start | bytes 786436
  184.9 4.3 %copy-start.15 = (f32[4,128,128]{2,1,0:T(8,128)S(1)}, f32[4,128,128]{2,1,0:T(8,128)}, u32[]{:S(2)}) copy-start(f32[4,128,128]{2,1,0:T(8,128)} %fusion.109) | copy-start | bytes 786436
  185.0 4.3 %copy-start.21 = (f32[4,128,128]{2,1,0:T(8,128)S(1)}, f32[4,128,128]{2,1,0:T(8,128)}, u32[]{:S(2)}) copy-start(f32[4,128,128]{2,1,0:T(8,128)} %copy-done.20) | copy-start | bytes 786436
  262.7 4.3 %copy-start.22 = (f32[32,128,128]{2,1,0:T(8,128)S(1)}, f32[32,128,128]{2,1,0:T(8,128)}, u32[]{:S(2)}) copy-start(f32[32,128,128]{2,1,0:T(8,128)} %all-gather.15.cloned.1.call-done) | copy-start | bytes 6291460
  271.4 17.7 %all-to-all-start.1 = ((bf16[32,2,2,4,128]{4,3,2,1,0:T(4,128)(2,1)}), bf16[32,2,2,4,128]{4,3,2,1,0:T(4,128)(2,1)}, u32[]{:S(2)}, u32[]{:S(2)}) async-start(bf16[32,2,2,4,128]{4,3,2,1,0:T(4,128)(2,1)} %bitcast.196), calls=%async_computation.1 | async-start | bytes 262144 | tf_op jit(solution)/shard_map/all_to_all | solution.py:42
  280.7 24.9 %copy-start.34 = (bf16[2,2,128]{2,1,0:T(2,128)(2,1)S(1)}, bf16[2,2,128]{2,1,0:T(2,128)(2,1)}, u32[]{:S(2)}) copy-start(bf16[2,2,128]{2,1,0:T(2,128)(2,1)} %param.29) | copy-start | bytes 3076
  280.7 24.9 %copy-start.35 = (f32[2,2]{1,0:T(2,128)S(1)}, f32[2,2]{1,0:T(2,128)}, u32[]{:S(2)}) copy-start(f32[2,2]{1,0:T(2,128)} %param.31) | copy-start | bytes 52
  280.7 25.1 %copy-start.37 = (f32[128]{0:T(128)S(1)}, f32[128]{0:T(128)}, u32[]{:S(2)}) copy-start(f32[128]{0:T(128)} %param.26) | copy-start | bytes 1540
  290.0 16.4 %copy-start.29 = (bf16[2,2,4,128]{3,2,1,0:T(4,128)(2,1)}, bf16[2,2,4,128]{3,2,1,0:T(4,128)(2,1)S(1)}, u32[]{:S(2)}) copy-start(bf16[2,2,4,128]{3,2,1,0:T(4,128)(2,1)S(1)} %reduce_sum.87) | copy-start | bytes 12292
  291.0 14.4 %all-to-all-start.2 = ((f32[32,1,1024]{2,1,0:T(1,128)}), f32[32,1,1024]{2,1,0:T(1,128)S(1)}, u32[]{:S(2)}, u32[]{:S(2)}) async-start(f32[32,1,1024]{2,1,0:T(1,128)} %broadcast_in_dim.80), calls=%async_computation.2 | async-start | bytes 262144 | tf_op jit(solution)/shard_map/all_to_all | solution.py:48
  (22 other events, 35.6 us)
Sparse Core Ops, SparseCore 0:
  122.8 26.8 all-gather.8
  151.5 27.0 all-gather.12
  180.3 41.2 all-gather.10
  223.2 39.4 all-gather.14
